TPU v7x, 32 devices: a whole 2x2x4 slice. The times are simulated.
32 devices in a mesh: fs: 8 (over z, y), tp: 4 (over x, core).
Axes of the slice: x: 2, y: 2, z: 4, core: 2. Of those that a mesh axis runs over, the one named last changes fastest.
Arguments:
- tokens: bfloat16 [4096, 2048], P(('fs', 'tp')), may hold values from -6 to 6
- norm_gain: float32 [2048], replicated, may hold values from 0.1 to 1.9
- up_weight: float32 [2048, 8192], P('fs', 'tp'), may hold values from -0.125 to 0.125
- down_weight: float32 [8192, 2048], P('tp', 'fs'), may hold values from -0.0625 to 0.0625
Outputs:
- mlp_out: bfloat16 [4096, 2048], P(('fs', 'tp'))
All inputs are finite; a program needn't handle non-finite values.
Results may differ from a plain program's by a relative error of at most 0.0017.
Values may be sent and summed in bfloat16 or wider, within the bound.
A program may use at most 64 MiB of HBM per device.

v0:
```python
import jax
import jax.numpy as jnp
from jax import lax
from jax.sharding import PartitionSpec as P

epsilon = 1e-06


def taken_in(slab, axis, dim, step, start):
    def gathered(part):
        return lax.all_gather(part, axis, axis=dim, tiled=True)

    return step(start, jax.tree.map(gathered, slab), jnp.int32(0))


def on_whole(shard, axis, dim, work):
    return work(lax.all_gather(shard, axis, axis=dim, tiled=True), jnp.int32(0))


def shards(tokens, norm_gain, up_weight, down_weight):
    values = tokens.astype(jnp.float32)
    scale = lax.rsqrt(jnp.mean(values * values, axis=-1, keepdims=True) + epsilon)
    normed = (values * scale * norm_gain).astype(jnp.bfloat16)
    grouped = lax.all_gather(normed, "tp", axis=0, tiled=True)
    empty = jnp.zeros((grouped.shape[0], up_weight.shape[1]), jnp.float32)

    def add_rows(total, piece, start):
        columns = lax.dynamic_slice_in_dim(grouped, start, piece.shape[0], 1)
        return total + jnp.dot(
            columns, piece.astype(jnp.bfloat16), preferred_element_type=jnp.float32
        )

    pre = taken_in(up_weight.astype(jnp.bfloat16), "fs", 0, add_rows, empty)
    hidden = jnp.square(jax.nn.relu(pre)).astype(jnp.bfloat16)

    def project(piece, start):
        return jnp.dot(hidden, piece.astype(jnp.bfloat16), preferred_element_type=jnp.float32)

    terms = on_whole(down_weight.astype(jnp.bfloat16), "fs", 1, project)
    summed = lax.psum_scatter(terms, "tp", scatter_dimension=0, tiled=True)
    return summed.astype(jnp.bfloat16)


def solution(mesh):
    placed = (P(("fs", "tp"), None), P(), P("fs", "tp"), P("tp", "fs"))
    return jax.shard_map(
        shards, mesh=mesh, in_specs=placed, out_specs=P(("fs", "tp"), None), check_vma=False
    )
```

profile of v0, /device:TPU:0, one launch (start us, length us, event | category | flops | bytes accessed | tf_op | source)
XLA Modules:
  0.0 355.4 jit_solution(4031330473352925980)
XLA Ops:
  6.5 0.0 copy-start
  6.5 0.0 all-gather.4.cloned.1.call-start
  6.5 1.4 fusion
  7.9 2.0 fusion.2
  10.0 0.0 all-gather.4.cloned.1.call-update
  10.0 0.0 all-gather.6.cloned.1.call-start
  10.0 2.7 convert_element_type.20
  12.7 0.0 all-gather.6.cloned.1.call-update
  12.8 0.0 all-gather.8.cloned.1.call-start
  12.8 0.0 copy-done
  12.8 1.1 convert_element_type.22
  14.0 0.0 all-gather.8.cloned.1.call-update
  14.0 0.0 reduce-scatter.2.cloned.1.call-start
  14.0 21.3 %all-gather.4.cloned.1.call-done = bf16[512,2048]{1,0:T(8,128)(2,1)} async-done(((bf16[128,2048]{1,0:T(8,128)(2,1)}), bf16[512,2048]{1,0:T(8,128)(2,1)}) %all-gather.4.cloned.1.call-update) | async-done | bytes 2097168 | tf_op jit(solution)/shard_map/all_gather | solution.py:24
  35.3 126.1 %all-gather.6.cloned.1.call-done = bf16[2048,2048]{1,0:T(8,128)(2,1)} async-done(((bf16[256,2048]{1,0:T(8,128)(2,1)}), bf16[2048,2048]{1,0:T(8,128)(2,1)}) %all-gather.6.cloned.1.call-update) | async-done | bytes 8388624 | tf_op jit(solution)/shard_map/all_gather | solution.py:11
  161.4 125.2 %all-gather.8.cloned.1.call-done = bf16[2048,2048]{1,0:T(8,128)(2,1)} async-done(((bf16[2048,256]{1,0:T(8,128)(2,1)}), bf16[2048,2048]{1,0:T(8,128)(2,1)}) %all-gather.8.cloned.1.call-update) | async-done | bytes 8388624 | tf_op jit(solution)/shard_map/all_gather | solution.py:17
  286.6 17.1 %fusion.3 = f32[512,2048]{1,0:T(8,128)} fusion(bf16[2048,2048]{1,0:T(8,128)(2,1)} %all-gather.8.cloned.1.call-done, bf16[512,2048]{1,0:T(8,128)(2,1)} %all-gather.4.cloned.1.call-done, bf16[2048,2048]{1,0:T(8,128)(2,1)} %all-gather.6.cloned.1.call-done), kind=kOutput, calls=%fused_computation.6 | convolution fusion | flops 8593080320 | bytes 23068672 | tf_op jit(solution)/shard_map/dot_general | solution.py:37
  303.7 0.0 reduce-scatter.2.cloned.1.call-update
  303.7 43.1 %reduce-scatter.2.cloned.1.call-done = f32[128,2048]{1,0:T(8,128)} async-done(((f32[512,2048]{1,0:T(8,128)}), f32[128,2048]{1,0:T(8,128)}) %reduce-scatter.2.cloned.1.call-update) | async-done | bytes 1048592 | tf_op jit(solution)/shard_map/reduce_scatter | solution.py:40
  346.8 2.1 convert_element_type.23
  (1 shorter events, 0.0 us)
Async XLA Ops:
  6.5 6.3 %copy-start = (f32[2048,256]{1,0:T(8,128)S(1)}, f32[2048,256]{1,0:T(8,128)}, u32[]{:S(2)}) copy-start(f32[2048,256]{1,0:T(8,128)} %param.7) | copy-start | bytes 6291460
  6.5 28.8 %all-gather.4.cloned.1.call-start = ((), (), s32[]{:S(2)}) async-start(), calls=%async_computation.1 | async-start | bytes 2621440 | tf_op jit(solution)/shard_map/all_gather | solution.py:24
  10.0 151.4 %all-gather.6.cloned.1.call-start = ((), (), s32[]{:S(2)}) async-start(), calls=%async_computation.2 | async-start | bytes 9437184 | tf_op jit(solution)/shard_map/all_gather | solution.py:11
  12.8 273.8 %all-gather.8.cloned.1.call-start = ((), (), s32[]{:S(2)}) async-start(), calls=%async_computation.3 | async-start | bytes 9437184 | tf_op jit(solution)/shard_map/all_gather | solution.py:17
  14.0 332.8 %reduce-scatter.2.cloned.1.call-start = ((), (), s32[]{:S(2)}) async-start(), calls=%async_computation.4 | async-start | bytes 5242880 | tf_op jit(solution)/shard_map/reduce_scatter | solution.py:40
Sparse Core Ops, SparseCore 0:
  10.1 25.1 all-gather.3
  37.5 123.9 all-gather.5
  163.5 123.0 all-gather.7
  303.9 42.9 reduce-scatter.1
where the time goes:
time: 356 us; the launch traced here: 355 us
  waiting for transfers between devices  316 us (89%)
  matrix products  17.1 us (5%)
  between operations  13.1 us (4%)
  other arithmetic  9.35 us (3%)
    all_gather x1, waiting for transfers between devices, gathered(): return lax.all_gather(part, axis, axis=dim, tiled=True)  126 us
    all_gather x1, waiting for transfers between devices, on_whole(): return work(lax.all_gather(shard, axis, axis=dim, tiled=True), jnp.int32(0))  125 us
    reduce_scatter x1, waiting for transfers between devices, shards(): summed = lax.psum_scatter(terms, 'tp', scatter_dimension=0, tiled=True)  43.1 us
    all_gather x1, waiting for transfers between devices, shards(): grouped = lax.all_gather(normed, 'tp', axis=0, tiled=True)  21.3 us
    dot_general x1, matrix products, project(): jnp.dot(hidden, piece.astype(jnp.bfloat16), preferred_element_type=jnp.fl...  17.1 us
  transfers between devices with their start and end apart: 4, of which 4 were waited for; matrix products, arithmetic and copies ran while one was open for 1% of the time, Pallas kernels for 0%

commit v1 on v0

v1 whole, which is shorter than its diff:
```python
import functools

import jax
import jax.numpy as jnp
from jax import lax
from jax.experimental import pallas as pl
from jax.experimental.pallas import tpu as pltpu
from jax.sharding import PartitionSpec as P

epsilon = 1e-06
MESH = pl.DeviceIdType.MESH
VMEM_LIMIT = 66_000_000


def shards(tokens, norm_gain, up_weight, down_weight):
    values = tokens.astype(jnp.float32)
    scale = lax.rsqrt(jnp.mean(values * values, axis=-1, keepdims=True) + epsilon)
    normed = (values * scale * norm_gain).astype(jnp.bfloat16)
    grouped = lax.all_gather(normed, "tp", axis=0, tiled=True)
    up = lax.all_gather(up_weight.astype(jnp.bfloat16), "fs", axis=0, tiled=True)
    pre = jnp.dot(grouped, up, preferred_element_type=jnp.float32)
    hidden = jnp.square(jax.nn.relu(pre)).astype(jnp.bfloat16)
    down = lax.all_gather(down_weight.astype(jnp.bfloat16), "fs", axis=1, tiled=True)
    terms = jnp.dot(hidden, down, preferred_element_type=jnp.float32)
    summed = lax.psum_scatter(terms, "tp", scatter_dimension=0, tiled=True)
    return summed.astype(jnp.bfloat16)


def kernel(
    nz, ny, nx, nc,
    tok_ref, gain_ref, up_ref, down_ref, out_ref,
    tok, up, down, up_out, down_out, hidden, own, s1, r1, s2, r2,
    tok_recv, tok_send, tok_pass, up_recv, up_send, up_cross, down_recv, down_send, down_cross,
    s1_send, r1_recv, s2_send, r2_recv,
):
    chips = ny * nx
    fs, tp = lax.axis_index("fs"), lax.axis_index("tp")
    z, y = fs // ny, lax.rem(fs, ny)
    x, c = tp // nc, lax.rem(tp, nc)
    other = 1 - c
    me = y * nx + x
    part = up.shape[2]
    width = down.shape[2]

    def at(zz, yy, xx, cc):
        return (zz * ny + yy, xx * nc + cc)

    def chip(step):
        place = lax.rem(me + step, chips)
        return place, place // nx, lax.rem(place, nx)

    def remote(src, dst, send, recv, to):
        return pltpu.make_async_remote_copy(
            src_ref=src, dst_ref=dst, send_sem=send, recv_sem=recv, device_id=to, device_id_type=MESH
        )

    barrier = pltpu.get_barrier_semaphore()

    def greet(to):
        pl.semaphore_signal(barrier, inc=1, device_id=to, device_id_type=MESH)

    for step in range(1, chips):
        _, yy, xx = chip(step)
        greet(at(z, yy, xx, c))
    greet(at(z, y, x, other))
    pl.when(z > 0)(lambda: greet(at(z - 1, y, x, c)))
    pl.when(z < nz - 1)(lambda: greet(at(z + 1, y, x, c)))

    mine = z * ny + y
    up[mine] = up_ref[:, pl.ds(pl.multiple_of(y * part, 128), part)].astype(jnp.bfloat16)
    for step in range(1, ny):
        yy = lax.rem(y + step, ny)
        up_out[step - 1] = up_ref[:, pl.ds(pl.multiple_of(yy * part, 128), part)].astype(jnp.bfloat16)
    values = tok_ref[...].astype(jnp.float32)
    scale = lax.rsqrt(jnp.mean(values * values, axis=-1, keepdims=True) + epsilon)
    tok[c * chips + me] = (values * scale * gain_ref[...]).astype(jnp.bfloat16)

    pl.semaphore_wait(
        barrier, chips + (z > 0).astype(jnp.int32) + (z < nz - 1).astype(jnp.int32)
    )

    def along(buf, send, recv, slot, step):
        to = z + step
        side = (step + 1) // 2
        return remote(buf.at[slot], buf.at[slot], send.at[slot, side], recv.at[slot], at(to, y, x, c))

    def pass_on(buf, send, recv, zz, slot, wait=False):
        def go(step):
            copy = along(buf, send, recv, slot, step)
            copy.wait_send() if wait else copy.start()

        pl.when((zz <= z) & (z < nz - 1))(lambda: go(1))
        pl.when((zz >= z) & (z > 0))(lambda: go(-1))

    def arrive(buf, send, recv, slot):
        along(buf, send, recv, slot, 1).wait_recv()

    def cross(buf, dst, send, recv, step):
        yy = lax.rem(y + step, ny)
        return remote(buf.at[step - 1], dst.at[mine], send.at[step - 1], recv.at[mine], at(z, yy, x, c))

    pass_on(up, up_send, up_recv, z, mine)
    for step in range(1, ny):
        cross(up_out, up, up_cross, up_recv, step).start()

    def tok_to(step):
        _, yy, xx = chip(step)
        slot = tok.at[c * chips + me]
        return remote(slot, slot, tok_send.at[step - 1], tok_recv.at[c * chips + me], at(z, yy, xx, c))

    def tok_over(place):
        slot = tok.at[c * chips + place]
        return remote(
            slot, slot, tok_pass.at[place], tok_recv.at[c * chips + place], at(z, y, x, other)
        )

    for step in range(1, chips):
        tok_to(step).start()
    tok_over(me).start()

    down[mine] = down_ref[pl.ds(pl.multiple_of(y * part, 128), part), :].astype(jnp.bfloat16)
    for step in range(1, ny):
        yy = lax.rem(y + step, ny)
        down_out[step - 1] = down_ref[pl.ds(pl.multiple_of(yy * part, 128), part), :].astype(jnp.bfloat16)
    for step in range(1, ny):
        cross(down_out, down, down_cross, down_recv, step).start()

    def rounds(count):
        return [(0, 0)] + [(d, s) for d in range(1, count) for s in (-1, 1)]

    for number, (distance, side) in enumerate(rounds(nz)):
        zz = z + side * distance

        @pl.when((zz >= 0) & (zz < nz))
        def _():
            for step in range(ny):
                slot = zz * ny + lax.rem(y + step, ny)
                if distance > 0 or step > 0:
                    arrive(up, up_send, up_recv, slot)
                    pass_on(up, up_send, up_recv, zz, slot)

        if number == 2:
            for step in range(1, chips):
                place, _, _ = chip(step)
                slot = tok.at[c * chips + place]
                remote(slot, slot, tok_send.at[step - 1], tok_recv.at[c * chips + place], at(z, y, x, other)).wait_recv()
                tok_over(place).start()

    pass_on(down, down_send, down_recv, z, mine)
    for step in range(1, ny):
        slot = z * ny + lax.rem(y + step, ny)
        arrive(down, down_send, down_recv, slot)
        pass_on(down, down_send, down_recv, z, slot)
    for place in range(chips):
        slot = tok.at[other * chips + place]
        remote(
            slot, slot, tok_pass.at[place], tok_recv.at[other * chips + place], at(z, y, x, other)
        ).wait_recv()

    rows = tok.shape[0] * tok.shape[1]
    depth = tok.shape[2]
    tile = 256

    def hide(n, carry):
        columns = pl.ds(pl.multiple_of(n * tile, tile), tile)
        pre = jnp.dot(
            tok[...].reshape(rows, depth),
            up[:, :, columns].reshape(depth, tile),
            preferred_element_type=jnp.float32,
        )
        hidden[:, columns] = jnp.square(jnp.maximum(pre, 0.0)).astype(jnp.bfloat16)
        return carry

    lax.fori_loop(0, part // tile, hide, 0)

    half = rows // nc
    shard = half // chips

    def to_core(slot):
        return remote(s1.at[slot], r1.at[slot], s1_send.at[slot], r1_recv.at[slot], at(z, y, x, other))

    def to_chip(slot, step):
        place, yy, xx = chip(step)
        return remote(
            s2.at[slot, place], r2.at[slot, step - 1], s2_send.at[slot, step - 1],
            r2_recv.at[slot, step - 1], at(z, yy, xx, c),
        )

    def project(zz, step):
        slot = zz * ny + lax.rem(y + step, ny)

        @pl.when(zz != z)
        def _():
            arrive(down, down_send, down_recv, slot)
            pass_on(down, down_send, down_recv, zz, slot)

        theirs = hidden[pl.ds(pl.multiple_of(other * half, half), half), :]
        s1[slot] = jnp.dot(theirs, down[slot], preferred_element_type=jnp.float32)
        to_core(slot).start()
        ours = hidden[pl.ds(pl.multiple_of(c * half, half), half), :]
        own[...] = jnp.dot(ours, down[slot], preferred_element_type=jnp.float32)
        to_core(slot).wait_recv()
        s2[slot] = (own[...] + r1[slot]).reshape(chips, shard, width)
        for hop in range(1, chips):
            to_chip(slot, hop).start()

    def take(number, carry):
        turn, step = number // ny, lax.rem(number, ny)
        distance = (turn + 1) // 2
        zz = jnp.where(lax.rem(turn, 2) == 1, z - distance, z + distance)
        pl.when((zz >= 0) & (zz < nz))(lambda: project(zz, step))
        return carry

    lax.fori_loop(0, (2 * nz - 1) * ny, take, 0)

    def finish(number, carry):
        turn, step = number // ny, lax.rem(number, ny)
        distance = (turn + 1) // 2
        zz = jnp.where(lax.rem(turn, 2) == 1, z - distance, z + distance)

        @pl.when((zz >= 0) & (zz < nz))
        def _():
            slot = zz * ny + lax.rem(y + step, ny)
            total = s2[slot, me]
            for hop in range(1, chips):
                to_chip(slot, hop).wait_recv()
                total = total + r2[slot, hop - 1]
            out_ref[:, pl.ds(pl.multiple_of(slot * width, 128), width)] = total.astype(jnp.bfloat16)
            to_core(slot).wait_send()
            for hop in range(1, chips):
                to_chip(slot, hop).wait_send()
            pass_on(up, up_send, up_recv, zz, slot, wait=True)
            pass_on(down, down_send, down_recv, zz, slot, wait=True)

        return carry

    lax.fori_loop(0, (2 * nz - 1) * ny, finish, 0)

    for step in range(1, ny):
        cross(up_out, up, up_cross, up_recv, step).wait_send()
        cross(down_out, down, down_cross, down_recv, step).wait_send()
    for step in range(1, chips):
        tok_to(step).wait_send()
    for place in range(chips):
        tok_over(place).wait_send()


def solution(mesh):
    fs, tp = mesh.shape["fs"], mesh.shape["tp"]
    ny = 1
    while (2 * ny) * (2 * ny) <= fs and fs % (2 * ny) == 0:
        ny *= 2
    nz, nc = fs // ny, 2
    nx = tp // nc
    chips = ny * nx
    placed = (P(("fs", "tp"), None), P(), P("fs", "tp"), P("tp", "fs"))

    def whole(tokens, norm_gain, up_weight, down_weight):
        rows, depth = tokens.shape
        share, span = up_weight.shape
        part, width = span // ny, down_weight.shape[1]
        held = chips * nc
        half = chips * rows
        vm, dma = pltpu.VMEM, pltpu.SemaphoreType.DMA
        low, full = jnp.bfloat16, jnp.float32
        shapes = [
            ((held, rows, depth), low), ((fs, share, part), low), ((fs, part, width), low),
            ((ny - 1, share, part), low), ((ny - 1, part, width), low), ((held * rows, part), low),
            ((half, width), full), ((fs, half, width), full), ((fs, half, width), full),
            ((fs, chips, rows, width), full), ((fs, chips - 1, rows, width), full),
        ]
        size = 0
        for shape, kind in shapes:
            count = 4 if kind == full else 2
            for extent in shape:
                count *= extent
            size += count
        size += 4 * (up_weight.size + down_weight.size) + 4 * tokens.size
        if size > VMEM_LIMIT * 9 // 10 or part % 256 or tp % nc or ny < 2 or chips < 2:
            return shards(tokens, norm_gain, up_weight, down_weight)
        at_vmem = pl.BlockSpec(memory_space=pltpu.VMEM)
        return pl.pallas_call(
            functools.partial(kernel, nz, ny, nx, nc),
            out_shape=jax.ShapeDtypeStruct((rows, depth), jnp.bfloat16),
            in_specs=[at_vmem] * 4,
            out_specs=at_vmem,
            scratch_shapes=[vm(shape, kind) for shape, kind in shapes] + [
                dma((held,)), dma((chips - 1,)), dma((chips,)),
                dma((fs,)), dma((fs, 2)), dma((ny - 1,)),
                dma((fs,)), dma((fs, 2)), dma((ny - 1,)),
                dma((fs,)), dma((fs,)), dma((fs, chips - 1)), dma((fs, chips - 1)),
            ],
            compiler_params=pltpu.CompilerParams(
                collective_id=0, has_side_effects=True, vmem_limit_bytes=VMEM_LIMIT
            ),
        )(tokens, norm_gain.reshape(1, depth), up_weight, down_weight)

    return jax.shard_map(
        whole, mesh=mesh, in_specs=placed, out_specs=P(("fs", "tp"), None), check_vma=False
    )
```

time: 356 us -> 173 us (0.49)
  waiting for transfers between devices: 316 us -> 0 us
  Pallas kernels: 0 us -> 169 us
  matrix products: 17.1 us -> 0 us
  between operations: 13.1 us -> 0.01 us
  other arithmetic: 9.35 us -> 0 us
    all_gather x3 -> x0, waiting for transfers between devices: 273 us -> none  [the longest x1 126 us: gathered(): return lax.all_gather(part, axis, axis=dim, tiled=True)]
    pallas_call x0 -> x1, Pallas kernels: none -> 169 us  [whole(): pl.pallas_call(functools.partial(kernel, nz, ny, nx, nc), out_shape=jax.S...]
    reduce_scatter x1 -> x0, waiting for transfers between devices: 43.1 us -> none  [shards(): summed = lax.psum_scatter(terms, 'tp', scatter_dimension=0, tiled=True)]
    dot_general x1 -> x0, matrix products: 17.1 us -> none  [project(): jnp.dot(hidden, piece.astype(jnp.bfloat16), preferred_element_type=jnp.fl...]
    convert_element_type x4 -> x0, other arithmetic: 7.96 us -> none  [the longest x1 2.71 us: shards(): pre = taken_in(up_weight.astype(jnp.bfloat16), 'fs', 0, add_rows, empty)]
  transfers between devices with their start and end apart: 4 -> 0, of which waited for: 4 -> 0; matrix products, arithmetic and copies ran while one was open for 1% -> 0% of each run, Pallas kernels for 0% -> 0%
where the time goes in v1:
time: 173 us; the launch traced here: 171 us
  Pallas kernels  169 us (98%)
  local copies, waits for them, and re-layouts  1.88 us (1%)
    pallas_call x1, Pallas kernels, whole(): pl.pallas_call(functools.partial(kernel, nz, ny, nx, nc), out_shape=jax.S...  169 us

profile of v1, /device:TPU:0, one launch (start us, length us, event | category | flops | bytes accessed | tf_op | source)
XLA Modules:
  0.0 171.3 jit_solution(12244347524676878518)
XLA Ops:
  0.0 169.4 %shard_map.46 = bf16[128,2048]{1,0:T(8,128)(2,1)} custom-call(bf16[128,2048]{1,0:T(8,128)(2,1)} %tok_ref.1, f32[1,2048]{1,0:T(1,128)} %bitcast.1, f32[256,2048]{1,0:T(8,128)} %up_ref.1, f32[2048,256]{1,0:T(8,128)} %down_ref.1), custom_call_target="tpu_custom_call" | custom-call | tf_op jit(solution)/shard_map/pallas_call | solution.py:282
  169.4 1.9 %copy.6 = bf16[128,2048]{1,0:T(8,128)(2,1)} copy(bf16[128,2048]{1,0:T(8,128)(2,1)} %shard_map.46) | data formatting | bytes 1048576

commit v2 on v1

--- a/solution.py
+++ b/solution.py
@@ -27,7 +27,7 @@
 
 
 def kernel(
-    nz, ny, nx, nc,
+    nz, ny, nx, nc, cuts,
     tok_ref, gain_ref, up_ref, down_ref, out_ref,
     tok, up, down, up_out, down_out, hidden, own, s1, r1, s2, r2,
     tok_recv, tok_send, tok_pass, up_recv, up_send, up_cross, down_recv, down_send, down_cross,
@@ -41,6 +41,8 @@
     me = y * nx + x
     part = up.shape[2]
     width = down.shape[2]
+    whole = width * cuts
+    outer = (z == 0) | (z == nz - 1)
 
     def at(zz, yy, xx, cc):
         return (zz * ny + yy, xx * nc + cc)
@@ -71,10 +73,6 @@
     for step in range(1, ny):
         yy = lax.rem(y + step, ny)
         up_out[step - 1] = up_ref[:, pl.ds(pl.multiple_of(yy * part, 128), part)].astype(jnp.bfloat16)
-    values = tok_ref[...].astype(jnp.float32)
-    scale = lax.rsqrt(jnp.mean(values * values, axis=-1, keepdims=True) + epsilon)
-    tok[c * chips + me] = (values * scale * gain_ref[...]).astype(jnp.bfloat16)
-
     pl.semaphore_wait(
         barrier, chips + (z > 0).astype(jnp.int32) + (z < nz - 1).astype(jnp.int32)
     )
@@ -99,9 +97,34 @@
         yy = lax.rem(y + step, ny)
         return remote(buf.at[step - 1], dst.at[mine], send.at[step - 1], recv.at[mine], at(z, yy, x, c))
 
+    def cross_down(step, cut):
+        yy = lax.rem(y + step, ny)
+        at_cut, to_cut = (step - 1) * cuts + cut, mine * cuts + cut
+        return remote(
+            down_out.at[at_cut], down.at[to_cut], down_cross.at[at_cut], down_recv.at[to_cut], at(z, yy, x, c)
+        )
+
+    def pass_down(slot):
+        for cut in range(cuts):
+            pass_on(down, down_send, down_recv, z, slot * cuts + cut)
+
     pass_on(up, up_send, up_recv, z, mine)
     for step in range(1, ny):
         cross(up_out, up, up_cross, up_recv, step).start()
+
+    values = tok_ref[...].astype(jnp.float32)
+    scale = lax.rsqrt(jnp.mean(values * values, axis=-1, keepdims=True) + epsilon)
+    tok[c * chips + me] = (values * scale * gain_ref[...]).astype(jnp.bfloat16)
+    for step in range(ny):
+        yy = lax.rem(y + step, ny)
+        for cut in range(cuts):
+            piece = down_ref[
+                pl.ds(pl.multiple_of(yy * part, 128), part), cut * width:(cut + 1) * width
+            ].astype(jnp.bfloat16)
+            if step == 0:
+                down[mine * cuts + cut] = piece
+            else:
+                down_out[(step - 1) * cuts + cut] = piece
 
     def tok_to(step):
         _, yy, xx = chip(step)
@@ -117,13 +140,17 @@
     for step in range(1, chips):
         tok_to(step).start()
     tok_over(me).start()
-
-    down[mine] = down_ref[pl.ds(pl.multiple_of(y * part, 128), part), :].astype(jnp.bfloat16)
+    pass_down(mine)
     for step in range(1, ny):
-        yy = lax.rem(y + step, ny)
-        down_out[step - 1] = down_ref[pl.ds(pl.multiple_of(yy * part, 128), part), :].astype(jnp.bfloat16)
-    for step in range(1, ny):
-        cross(down_out, down, down_cross, down_recv, step).start()
+        for cut in range(cuts):
+            cross_down(step, cut).start()
+
+    def take_crossed():
+        for step in range(1, ny):
+            slot = z * ny + lax.rem(y + step, ny)
+            for cut in range(cuts):
+                arrive(down, down_send, down_recv, slot * cuts + cut)
+            pass_down(slot)
 
     def rounds(count):
         return [(0, 0)] + [(d, s) for d in range(1, count) for s in (-1, 1)]
@@ -145,12 +172,9 @@
                 slot = tok.at[c * chips + place]
                 remote(slot, slot, tok_send.at[step - 1], tok_recv.at[c * chips + place], at(z, y, x, other)).wait_recv()
                 tok_over(place).start()
-
-    pass_on(down, down_send, down_recv, z, mine)
-    for step in range(1, ny):
-        slot = z * ny + lax.rem(y + step, ny)
-        arrive(down, down_send, down_recv, slot)
-        pass_on(down, down_send, down_recv, z, slot)
+            pl.when(outer)(take_crossed)
+
+    pl.when(~outer)(take_crossed)
     for place in range(chips):
         slot = tok.at[other * chips + place]
         remote(
@@ -186,9 +210,13 @@
             r2_recv.at[slot, step - 1], at(z, yy, xx, c),
         )
 
-    def project(zz, step):
-        slot = zz * ny + lax.rem(y + step, ny)
-
+    def blocks(number):
+        turn, rest = number // (ny * cuts), lax.rem(number, ny * cuts)
+        distance = (turn + 1) // 2
+        zz = jnp.where(lax.rem(turn, 2) == 1, z - distance, z + distance)
+        return zz, zz * ny + lax.rem(y + rest // cuts, ny), lax.rem(rest, cuts)
+
+    def project(zz, slot):
         @pl.when(zz != z)
         def _():
             arrive(down, down_send, down_recv, slot)
@@ -205,22 +233,18 @@
             to_chip(slot, hop).start()
 
     def take(number, carry):
-        turn, step = number // ny, lax.rem(number, ny)
-        distance = (turn + 1) // 2
-        zz = jnp.where(lax.rem(turn, 2) == 1, z - distance, z + distance)
-        pl.when((zz >= 0) & (zz < nz))(lambda: project(zz, step))
+        zz, slot, cut = blocks(number)
+        pl.when((zz >= 0) & (zz < nz))(lambda: project(zz, slot * cuts + cut))
         return carry
 
-    lax.fori_loop(0, (2 * nz - 1) * ny, take, 0)
+    lax.fori_loop(0, (2 * nz - 1) * ny * cuts, take, 0)
 
     def finish(number, carry):
-        turn, step = number // ny, lax.rem(number, ny)
-        distance = (turn + 1) // 2
-        zz = jnp.where(lax.rem(turn, 2) == 1, z - distance, z + distance)
+        zz, first, cut = blocks(number)
 
         @pl.when((zz >= 0) & (zz < nz))
         def _():
-            slot = zz * ny + lax.rem(y + step, ny)
+            slot = first * cuts + cut
             total = s2[slot, me]
             for hop in range(1, chips):
                 to_chip(slot, hop).wait_recv()
@@ -229,16 +253,17 @@
             to_core(slot).wait_send()
             for hop in range(1, chips):
                 to_chip(slot, hop).wait_send()
-            pass_on(up, up_send, up_recv, zz, slot, wait=True)
             pass_on(down, down_send, down_recv, zz, slot, wait=True)
+            pl.when(cut == 0)(lambda: pass_on(up, up_send, up_recv, zz, first, wait=True))
 
         return carry
 
-    lax.fori_loop(0, (2 * nz - 1) * ny, finish, 0)
+    lax.fori_loop(0, (2 * nz - 1) * ny * cuts, finish, 0)
 
     for step in range(1, ny):
         cross(up_out, up, up_cross, up_recv, step).wait_send()
-        cross(down_out, down, down_cross, down_recv, step).wait_send()
+        for cut in range(cuts):
+            cross_down(step, cut).wait_send()
     for step in range(1, chips):
         tok_to(step).wait_send()
     for place in range(chips):
@@ -252,22 +277,23 @@
         ny *= 2
     nz, nc = fs // ny, 2
     nx = tp // nc
-    chips = ny * nx
+    chips, cuts = ny * nx, 2
     placed = (P(("fs", "tp"), None), P(), P("fs", "tp"), P("tp", "fs"))
 
     def whole(tokens, norm_gain, up_weight, down_weight):
         rows, depth = tokens.shape
         share, span = up_weight.shape
-        part, width = span // ny, down_weight.shape[1]
+        part, width = span // ny, down_weight.shape[1] // cuts
+        pieces = fs * cuts
         held = chips * nc
         half = chips * rows
         vm, dma = pltpu.VMEM, pltpu.SemaphoreType.DMA
         low, full = jnp.bfloat16, jnp.float32
         shapes = [
-            ((held, rows, depth), low), ((fs, share, part), low), ((fs, part, width), low),
-            ((ny - 1, share, part), low), ((ny - 1, part, width), low), ((held * rows, part), low),
-            ((half, width), full), ((fs, half, width), full), ((fs, half, width), full),
-            ((fs, chips, rows, width), full), ((fs, chips - 1, rows, width), full),
+            ((held, rows, depth), low), ((fs, share, part), low), ((pieces, part, width), low),
+            ((ny - 1, share, part), low), (((ny - 1) * cuts, part, width), low), ((held * rows, part), low),
+            ((half, width), full), ((pieces, half, width), full), ((pieces, half, width), full),
+            ((pieces, chips, rows, width), full), ((pieces, chips - 1, rows, width), full),
         ]
         size = 0
         for shape, kind in shapes:
@@ -276,19 +302,19 @@
                 count *= extent
             size += count
         size += 4 * (up_weight.size + down_weight.size) + 4 * tokens.size
-        if size > VMEM_LIMIT * 9 // 10 or part % 256 or tp % nc or ny < 2 or chips < 2:
+        if size > VMEM_LIMIT * 9 // 10 or part % 256 or width % 128 or tp % nc or ny < 2 or chips < 2:
             return shards(tokens, norm_gain, up_weight, down_weight)
         at_vmem = pl.BlockSpec(memory_space=pltpu.VMEM)
         return pl.pallas_call(
-            functools.partial(kernel, nz, ny, nx, nc),
+            functools.partial(kernel, nz, ny, nx, nc, cuts),
             out_shape=jax.ShapeDtypeStruct((rows, depth), jnp.bfloat16),
             in_specs=[at_vmem] * 4,
             out_specs=at_vmem,
             scratch_shapes=[vm(shape, kind) for shape, kind in shapes] + [
                 dma((held,)), dma((chips - 1,)), dma((chips,)),
                 dma((fs,)), dma((fs, 2)), dma((ny - 1,)),
-                dma((fs,)), dma((fs, 2)), dma((ny - 1,)),
-                dma((fs,)), dma((fs,)), dma((fs, chips - 1)), dma((fs, chips - 1)),
+                dma((pieces,)), dma((pieces, 2)), dma(((ny - 1) * cuts,)),
+                dma((pieces,)), dma((pieces,)), dma((pieces, chips - 1)), dma((pieces, chips - 1)),
             ],
             compiler_params=pltpu.CompilerParams(
                 collective_id=0, has_side_effects=True, vmem_limit_bytes=VMEM_LIMIT

time: 173 us -> 156 us (0.902)
  Pallas kernels: 169 us -> 154 us
    pallas_call x1, Pallas kernels: 169 us -> 154 us  [whole(): pl.pallas_call(functools.partial(kernel, nz, ny, nx, nc, cuts), out_shape...]
where the time goes in v2:
time: 156 us
  Pallas kernels  154 us (99%)
  local copies, waits for them, and re-layouts  1.88 us (1%)
    pallas_call x1, Pallas kernels, whole(): pl.pallas_call(functools.partial(kernel, nz, ny, nx, nc, cuts), out_shape...  154 us

profile of v2, /device:TPU:0, one launch (start us, length us, event | category | flops | bytes accessed | tf_op | source)
XLA Modules:
  0.0 155.6 jit_solution(11025865668509171860)
XLA Ops:
  0.0 153.7 %shard_map.46 = bf16[128,2048]{1,0:T(8,128)(2,1)} custom-call(bf16[128,2048]{1,0:T(8,128)(2,1)} %tok_ref.1, f32[1,2048]{1,0:T(1,128)} %bitcast.1, f32[256,2048]{1,0:T(8,128)} %up_ref.1, f32[2048,256]{1,0:T(8,128)} %down_ref.1), custom_call_target="tpu_custom_call" | custom-call | tf_op jit(solution)/shard_map/pallas_call | solution.py:308
  153.7 1.9 %copy.6 = bf16[128,2048]{1,0:T(8,128)(2,1)} copy(bf16[128,2048]{1,0:T(8,128)(2,1)} %shard_map.46) | data formatting | bytes 1048576

commit v3 on v2

--- a/solution.py
+++ b/solution.py
@@ -29,9 +29,9 @@
 def kernel(
     nz, ny, nx, nc, cuts,
     tok_ref, gain_ref, up_ref, down_ref, out_ref,
-    tok, up, down, up_out, down_out, hidden, own, s1, r1, s2, r2,
+    tok, up, down, up_out, down_out, hidden, up_in, down_in, s1, r1, s2, r2,
     tok_recv, tok_send, tok_pass, up_recv, up_send, up_cross, down_recv, down_send, down_cross,
-    s1_send, r1_recv, s2_send, r2_recv,
+    s1_send, r1_recv, s2_send, r2_recv, load,
 ):
     chips = ny * nx
     fs, tp = lax.axis_index("fs"), lax.axis_index("tp")
@@ -41,7 +41,6 @@
     me = y * nx + x
     part = up.shape[2]
     width = down.shape[2]
-    whole = width * cuts
     outer = (z == 0) | (z == nz - 1)
 
     def at(zz, yy, xx, cc):
@@ -69,10 +68,27 @@
     pl.when(z < nz - 1)(lambda: greet(at(z + 1, y, x, c)))
 
     mine = z * ny + y
-    up[mine] = up_ref[:, pl.ds(pl.multiple_of(y * part, 128), part)].astype(jnp.bfloat16)
-    for step in range(1, ny):
-        yy = lax.rem(y + step, ny)
-        up_out[step - 1] = up_ref[:, pl.ds(pl.multiple_of(yy * part, 128), part)].astype(jnp.bfloat16)
+
+    def piece_of(step):
+        return pl.ds(pl.multiple_of(lax.rem(y + step, ny) * part, 128), part)
+
+    def load_up(step):
+        return pltpu.make_async_copy(
+            up_ref.at[:, piece_of(step)], up_in.at[:, piece_of(step)], load.at[step]
+        )
+
+    load_down = pltpu.make_async_copy(down_ref, down_in, load.at[ny])
+    for step in range(ny):
+        load_up(step).start()
+    load_down.start()
+    for step in range(ny):
+        load_up(step).wait()
+        piece = up_in[:, piece_of(step)].astype(jnp.bfloat16)
+        if step == 0:
+            up[mine] = piece
+        else:
+            up_out[step - 1] = piece
+
     pl.semaphore_wait(
         barrier, chips + (z > 0).astype(jnp.int32) + (z < nz - 1).astype(jnp.int32)
     )
@@ -104,8 +120,8 @@
             down_out.at[at_cut], down.at[to_cut], down_cross.at[at_cut], down_recv.at[to_cut], at(z, yy, x, c)
         )
 
-    def pass_down(slot):
-        for cut in range(cuts):
+    def pass_down(slot, first=0, last=cuts):
+        for cut in range(first, last):
             pass_on(down, down_send, down_recv, z, slot * cuts + cut)
 
     pass_on(up, up_send, up_recv, z, mine)
@@ -115,11 +131,11 @@
     values = tok_ref[...].astype(jnp.float32)
     scale = lax.rsqrt(jnp.mean(values * values, axis=-1, keepdims=True) + epsilon)
     tok[c * chips + me] = (values * scale * gain_ref[...]).astype(jnp.bfloat16)
+    load_down.wait()
     for step in range(ny):
-        yy = lax.rem(y + step, ny)
         for cut in range(cuts):
-            piece = down_ref[
-                pl.ds(pl.multiple_of(yy * part, 128), part), cut * width:(cut + 1) * width
+            piece = down_in[
+                piece_of(step), cut * width:(cut + 1) * width
             ].astype(jnp.bfloat16)
             if step == 0:
                 down[mine * cuts + cut] = piece
@@ -141,9 +157,6 @@
         tok_to(step).start()
     tok_over(me).start()
     pass_down(mine)
-    for step in range(1, ny):
-        for cut in range(cuts):
-            cross_down(step, cut).start()
 
     def take_crossed():
         for step in range(1, ny):
@@ -166,6 +179,10 @@
                     arrive(up, up_send, up_recv, slot)
                     pass_on(up, up_send, up_recv, zz, slot)
 
+        if number == 0:
+            for step in range(1, ny):
+                for cut in range(cuts):
+                    cross_down(step, cut).start()
         if number == 2:
             for step in range(1, chips):
                 place, _, _ = chip(step)
@@ -210,14 +227,16 @@
             r2_recv.at[slot, step - 1], at(z, yy, xx, c),
         )
 
+    far = jnp.where(z >= nz // 2, -1, 1)
+    reach = jnp.where(z >= nz // 2, z, nz - 1 - z)
+
     def blocks(number):
         turn, rest = number // (ny * cuts), lax.rem(number, ny * cuts)
-        distance = (turn + 1) // 2
-        zz = jnp.where(lax.rem(turn, 2) == 1, z - distance, z + distance)
+        zz = z + jnp.where(turn <= reach, far * turn, far * (reach - turn))
         return zz, zz * ny + lax.rem(y + rest // cuts, ny), lax.rem(rest, cuts)
 
     def project(zz, slot):
-        @pl.when(zz != z)
+        @pl.when((jnp.abs(zz - z) > 1) | (outer & (zz != z)))
         def _():
             arrive(down, down_send, down_recv, slot)
             pass_on(down, down_send, down_recv, zz, slot)
@@ -226,39 +245,65 @@
         s1[slot] = jnp.dot(theirs, down[slot], preferred_element_type=jnp.float32)
         to_core(slot).start()
         ours = hidden[pl.ds(pl.multiple_of(c * half, half), half), :]
-        own[...] = jnp.dot(ours, down[slot], preferred_element_type=jnp.float32)
+        s2[slot] = jnp.dot(ours, down[slot], preferred_element_type=jnp.float32).reshape(chips, shard, width)
+
+    def spread(number):
+        _, first, cut = blocks(number)
+        slot = first * cuts + cut
         to_core(slot).wait_recv()
-        s2[slot] = (own[...] + r1[slot]).reshape(chips, shard, width)
+        s2[slot] = s2[slot] + r1[slot].reshape(chips, shard, width)
         for hop in range(1, chips):
             to_chip(slot, hop).start()
 
+    def finish(number):
+        _, first, cut = blocks(number)
+        slot = first * cuts + cut
+        total = s2[slot, me]
+        for hop in range(1, chips):
+            to_chip(slot, hop).wait_recv()
+            total = total + r2[slot, hop - 1]
+        out_ref[:, pl.ds(pl.multiple_of(slot * width, 128), width)] = total.astype(jnp.bfloat16)
+
+    def hand_on(side):
+        for piece in range(ny * cuts):
+            slot = ((z + side) * ny + lax.rem(y + piece // cuts, ny)) * cuts + piece % cuts
+            arrive(down, down_send, down_recv, slot)
+            pass_on(down, down_send, down_recv, z + side, slot)
+
+    @pl.when(~outer)
+    def _():
+        for side in (-1, 1):
+            hand_on(side)
+
+    steps, late = nz * ny * cuts, 4
+
     def take(number, carry):
         zz, slot, cut = blocks(number)
-        pl.when((zz >= 0) & (zz < nz))(lambda: project(zz, slot * cuts + cut))
+        project(zz, slot * cuts + cut)
+        pl.when(number >= 1)(lambda: spread(number - 1))
+        pl.when(number >= late)(lambda: finish(number - late))
         return carry
 
-    lax.fori_loop(0, (2 * nz - 1) * ny * cuts, take, 0)
-
-    def finish(number, carry):
+    lax.fori_loop(0, steps, take, 0)
+    spread(steps - 1)
+
+    def close(number, carry):
+        finish(number)
+        return carry
+
+    lax.fori_loop(steps - late, steps, close, 0)
+
+    def settle(number, carry):
         zz, first, cut = blocks(number)
-
-        @pl.when((zz >= 0) & (zz < nz))
-        def _():
-            slot = first * cuts + cut
-            total = s2[slot, me]
-            for hop in range(1, chips):
-                to_chip(slot, hop).wait_recv()
-                total = total + r2[slot, hop - 1]
-            out_ref[:, pl.ds(pl.multiple_of(slot * width, 128), width)] = total.astype(jnp.bfloat16)
-            to_core(slot).wait_send()
-            for hop in range(1, chips):
-                to_chip(slot, hop).wait_send()
-            pass_on(down, down_send, down_recv, zz, slot, wait=True)
-            pl.when(cut == 0)(lambda: pass_on(up, up_send, up_recv, zz, first, wait=True))
-
+        slot = first * cuts + cut
+        to_core(slot).wait_send()
+        for hop in range(1, chips):
+            to_chip(slot, hop).wait_send()
+        pass_on(down, down_send, down_recv, zz, slot, wait=True)
+        pl.when(cut == 0)(lambda: pass_on(up, up_send, up_recv, zz, first, wait=True))
         return carry
 
-    lax.fori_loop(0, (2 * nz - 1) * ny * cuts, finish, 0)
+    lax.fori_loop(0, steps, settle, 0)
 
     for step in range(1, ny):
         cross(up_out, up, up_cross, up_recv, step).wait_send()
@@ -292,7 +337,7 @@
         shapes = [
             ((held, rows, depth), low), ((fs, share, part), low), ((pieces, part, width), low),
             ((ny - 1, share, part), low), (((ny - 1) * cuts, part, width), low), ((held * rows, part), low),
-            ((half, width), full), ((pieces, half, width), full), ((pieces, half, width), full),
+            ((share, span), full), ((span, width * cuts), full), ((pieces, half, width), full), ((pieces, half, width), full),
             ((pieces, chips, rows, width), full), ((pieces, chips - 1, rows, width), full),
         ]
         size = 0
@@ -301,20 +346,20 @@
             for extent in shape:
                 count *= extent
             size += count
-        size += 4 * (up_weight.size + down_weight.size) + 4 * tokens.size
-        if size > VMEM_LIMIT * 9 // 10 or part % 256 or width % 128 or tp % nc or ny < 2 or chips < 2:
+        size += 4 * tokens.size
+        if size > VMEM_LIMIT * 9 // 10 or part % 256 or width % 128 or tp % nc or ny < 2 or chips < 2 or nz > 4:
             return shards(tokens, norm_gain, up_weight, down_weight)
         at_vmem = pl.BlockSpec(memory_space=pltpu.VMEM)
         return pl.pallas_call(
             functools.partial(kernel, nz, ny, nx, nc, cuts),
             out_shape=jax.ShapeDtypeStruct((rows, depth), jnp.bfloat16),
-            in_specs=[at_vmem] * 4,
+            in_specs=[at_vmem] * 2 + [pl.BlockSpec(memory_space=pl.ANY)] * 2,
             out_specs=at_vmem,
             scratch_shapes=[vm(shape, kind) for shape, kind in shapes] + [
                 dma((held,)), dma((chips - 1,)), dma((chips,)),
                 dma((fs,)), dma((fs, 2)), dma((ny - 1,)),
                 dma((pieces,)), dma((pieces, 2)), dma(((ny - 1) * cuts,)),
-                dma((pieces,)), dma((pieces,)), dma((pieces, chips - 1)), dma((pieces, chips - 1)),
+                dma((pieces,)), dma((pieces,)), dma((pieces, chips - 1)), dma((pieces, chips - 1)), dma((ny + 1,)),
             ],
             compiler_params=pltpu.CompilerParams(
                 collective_id=0, has_side_effects=True, vmem_limit_bytes=VMEM_LIMIT

time: 156 us -> 156 us (level)
  no operation moved by 1% of the time
where the time goes in v3:
time: 156 us
  Pallas kernels  154 us (99%)
  local copies, waits for them, and re-layouts  1.88 us (1%)
    pallas_call x1, Pallas kernels, whole(): pl.pallas_call(functools.partial(kernel, nz, ny, nx, nc, cuts), out_shape...  154 us

profile of v3, /device:TPU:0, one launch (start us, length us, event | category | flops | bytes accessed | tf_op | source)
XLA Modules:
  0.0 156.0 jit_solution(602210270686494966)
XLA Ops:
  0.0 154.1 %shard_map.46 = bf16[128,2048]{1,0:T(8,128)(2,1)} custom-call(bf16[128,2048]{1,0:T(8,128)(2,1)} %tok_ref.1, f32[1,2048]{1,0:T(1,128)} %bitcast.1, f32[256,2048]{1,0:T(8,128)} %up_ref.1, f32[2048,256]{1,0:T(8,128)} %down_ref.1), custom_call_target="tpu_custom_call" | custom-call | tf_op jit(solution)/shard_map/pallas_call | solution.py:353
  154.1 1.9 %copy.6 = bf16[128,2048]{1,0:T(8,128)(2,1)} copy(bf16[128,2048]{1,0:T(8,128)(2,1)} %shard_map.46) | data formatting | bytes 1048576
